TPU v7x, 32 devices: a whole 2x2x4 slice. The times are simulated.
32 devices in a mesh: grp: 2 (over x), ep: 16 (over z, y, core).
Axes of the slice: x: 2, y: 2, z: 4, core: 2. Of those that a mesh axis runs over, the one named last changes fastest.
Arguments:
- tokens: bfloat16 [4096, 2048], P(('grp', 'ep')), parts along dimension 0, may hold values from -6 to 6
- routing: int32 [4096, 2], P(('grp', 'ep')), parts along dimension 0, may hold values from 0 to 3, all different within a row; in each aligned block of 128 rows (0 to 127, 128 to 255, ...) at most 80 rows name the same one
- gates: float32 [4096, 2], P(('grp', 'ep')), parts along dimension 0, may hold values from 0.2 to 1
- norm_gain: bfloat16 [2048], replicated, may hold values from 0.099609375 to 1.8984375
- w_gate: bfloat16 [16, 2048, 896], P('ep'), may hold values from -0.125 to 0.125
- w_up: bfloat16 [16, 2048, 896], P('ep'), may hold values from -0.125 to 0.125
- w_down: bfloat16 [16, 896, 2048], P('ep'), may hold values from -0.09375 to 0.09375
Outputs:
- mixed: bfloat16 [4096, 2048], P(('grp', 'ep')), parts along dimension 0
There are 2 independent parts, one for each index of `grp`. A program takes and returns all parts, laid end to end along the dimension named above; an argument that names none is the same for every part. Nothing has to cross between parts.
Inputs may be any that keep to these rules, and one draw needn't show every extreme that they name: `routing`: each row names 2 different experts. Among the rows of one device at most 80 name any one expert, and in every draw some expert is named by exactly 80 rows of some device.
All inputs are finite; a program needn't handle non-finite values.
Results may differ from a plain program's by a relative error of at most 0.0078.
Values may be sent and summed in bfloat16 or wider, within the bound.
A program may use at most 128 MiB of HBM per device.

v0:
```python
import jax
import jax.numpy as jnp
from jax import lax
from jax.sharding import PartitionSpec as P

GROUP = 4


def partner(x, axis, distance):
    return lax.ppermute(x, axis, [(i, i ^ 1 << distance) for i in range(lax.axis_size(axis))])


def per_device(tokens, routing, gates, norm_gain, w_gate, w_up, w_down):
    tok_count, model_width = tokens.shape
    top_count = routing.shape[1]
    devices = lax.axis_size("ep")
    experts = devices // GROUP
    member_slots = 5 * tok_count * top_count // (4 * devices)
    capacity = GROUP * member_slots
    group_bits = GROUP.bit_length() - 1
    own_index = lax.axis_index("ep")
    values = tokens.astype(jnp.float32)
    scale = lax.rsqrt(jnp.mean(values * values, axis=-1, keepdims=True) + 1e-06)
    normed = (values * scale * norm_gain.astype(jnp.float32)).astype(jnp.bfloat16)
    one_hot = (routing[..., None] == jnp.arange(experts, dtype=jnp.int32)).astype(jnp.int32)
    per_token = jnp.sum(one_hot, axis=1)
    before = jnp.cumsum(per_token, axis=0) - per_token
    slots = jnp.sum(one_hot * before[:, None, :], axis=-1)
    target = (routing * capacity + slots).reshape(-1)
    outgoing = jnp.zeros((experts * capacity, model_width), jnp.bfloat16)
    outgoing = outgoing.at[target].set(jnp.repeat(normed, top_count, axis=0))
    copies = jnp.broadcast_to(
        outgoing.reshape(experts, 1, capacity, model_width), (experts, GROUP, capacity, model_width)
    )
    arrived = lax.all_to_all(
        copies.reshape(devices, capacity, model_width),
        "ep",
        split_axis=0,
        concat_axis=0,
        tiled=True,
    )
    expert_rows = arrived.reshape(devices * capacity, model_width)
    gate_act = jnp.dot(expert_rows, w_gate[0], preferred_element_type=jnp.float32)
    up_act = jnp.dot(expert_rows, w_up[0], preferred_element_type=jnp.float32)
    hidden = (jax.nn.silu(gate_act) * up_act).astype(jnp.bfloat16)
    partial_value = jnp.dot(hidden, w_down[0], preferred_element_type=jnp.float32)
    summed = partial_value.reshape(devices, GROUP, member_slots, model_width)
    for bit_index in range(group_bits):
        halves = summed.reshape(devices, summed.shape[1] // 2, 2, member_slots, model_width)
        own_bit = own_index >> bit_index & 1
        kept_part = lax.dynamic_index_in_dim(halves, own_bit, 2, keepdims=False)
        given_part = lax.dynamic_index_in_dim(halves, 1 - own_bit, 2, keepdims=False)
        summed = kept_part + partner(given_part, "ep", bit_index)
    finished = summed.reshape(devices, member_slots, model_width).astype(jnp.bfloat16)
    returned = lax.all_to_all(finished, "ep", split_axis=0, concat_axis=0, tiled=True)
    picked = returned.reshape(experts * capacity, model_width)[target]
    picked = picked.reshape(tok_count, top_count, model_width)
    mixed = jnp.sum(gates[..., None] * picked.astype(jnp.float32), axis=1)
    return mixed.astype(jnp.bfloat16)


def solution(mesh):
    placed = (
        P(("grp", "ep"), None),
        P(("grp", "ep"), None),
        P(("grp", "ep"), None),
        P(),
        P("ep", None, None),
        P("ep", None, None),
        P("ep", None, None),
    )
    return jax.shard_map(
        per_device, mesh=mesh, in_specs=placed, out_specs=P(("grp", "ep"), None), check_vma=False
    )
```

profile of v0, /device:TPU:13, one launch (start us, length us, event | category | flops | bytes accessed | tf_op | source)
XLA Modules:
  0.0 312.1 jit_solution(14940660908148093949)
XLA Ops:
  3.4 1.2 fusion.6
  4.6 1.2 fusion.8
  7.0 2.5 scatter_custom_fusion
  9.5 3.0 broadcast_in_dim.11
  12.5 6.5 %all-to-all-start = ((bf16[16,80,2048]{2,1,0:T(8,128)(2,1)}), bf16[16,80,2048]{2,1,0:T(8,128)(2,1)}, u32[]{:S(2)}, u32[]{:S(2)}) async-start(bf16[16,80,2048]{2,1,0:T(8,128)(2,1)} %bitcast.27), calls=%async_computation | async-start | bytes 10485760 | tf_op jit(solution)/shard_map/all_to_all | solution.py:35
  19.0 114.9 %all-to-all-done = bf16[16,80,2048]{2,1,0:T(8,128)(2,1)} async-done(((bf16[16,80,2048]{2,1,0:T(8,128)(2,1)}), bf16[16,80,2048]{2,1,0:T(8,128)(2,1)}, u32[]{:S(2)}, u32[]{:S(2)}) %all-to-all-start) | async-done | bytes 5242912 | tf_op jit(solution)/shard_map/all_to_all | solution.py:35
  133.9 8.7 %fusion.3 = f32[1280,896]{1,0:T(8,128)S(1)} fusion(bf16[1280,2048]{1,0:T(8,128)(2,1)} %bitcast.3, bf16[1,2048,896]{2,1,0:T(8,128)(2,1)} %param.11), kind=kOutput, calls=%fused_computation.8 | convolution fusion | flops 4697620480 | bytes 13500416 | tf_op jit(solution)/shard_map/dot_general | solution.py:43
  142.7 8.8 %multiply_convert_fusion = bf16[1280,896]{1,0:T(8,128)(2,1)} fusion(f32[1280,896]{1,0:T(8,128)S(1)} %fusion.3, bf16[1280,2048]{1,0:T(8,128)(2,1)} %bitcast.3, bf16[1,2048,896]{2,1,0:T(8,128)(2,1)S(1)} %copy-done.2), kind=kOutput, calls=%fused_computation.4 | convolution fusion | flops 4704501760 | bytes 15794176 | tf_op jit(solution)/shard_map/dot_general | solution.py:44
  151.5 3.4 %dot_general.13 = bf16[16,2,2,20,896]{4,3,2,1,0:T(8,128)(2,1)S(1)} reshape(bf16[1280,896]{1,0:T(8,128)(2,1)} %multiply_convert_fusion) | data formatting | bytes 4587520 | tf_op jit(solution)/shard_map/dot_general | solution.py:46
  154.8 11.1 %fusion = f32[16,2,2,20,2048]{4,3,2,1,0:T(8,128)} fusion(bf16[16,2,2,20,896]{4,3,2,1,0:T(8,128)(2,1)S(1)} %dot_general.13, bf16[1,896,2048]{2,1,0:T(8,128)(2,1)} %param.13), kind=kOutput, calls=%fused_computation.5 | convolution fusion | flops 4697620480 | bytes 16449536 | tf_op jit(solution)/shard_map/dot_general | solution.py:46
  166.0 8.8 %constant_dynamic-slice_fusion.1 = (f32[16,2,1,20,2048]{4,3,2,1,0:T(8,128)}, f32[16,2,1,20,2048]{4,3,2,1,0:T(8,128)S(1)}) fusion(f32[16,2,2,20,2048]{4,3,2,1,0:T(8,128)} %fusion, s32[]{:T(128)S(6)} %select_n.26, s32[]{:T(128)S(6)} %select_n.27), kind=kLoop, calls=%fused_computation.26 | loop fusion | bytes 20971528 | tf_op jit(solution)/shard_map/jit(dynamic_index_in_dim)/dynamic_slice | solution.py:51
  174.8 5.4 %copy.36 = f32[16,2,1,20,2048]{4,0,3,2,1:T(8,128)} copy(f32[16,2,1,20,2048]{4,3,2,1,0:T(8,128)S(1)} %get-tuple-element.6) | data formatting | bytes 10485760 | tf_op jit(solution)/shard_map/jit(dynamic_index_in_dim)/dynamic_slice | solution.py:52
  180.3 8.9 %collective-permute-done = f32[16,2,20,2048]{3,0,2,1:T(8,128)} collective-permute-done((f32[16,2,20,2048]{3,0,2,1:T(8,128)}, f32[16,2,20,2048]{3,0,2,1:T(8,128)}, u32[]{:S(2)}, u32[]{:S(2)}) %collective-permute-start) | collective-permute-done | bytes 5242912 | tf_op jit(solution)/shard_map/ppermute | solution.py:10
  189.2 7.7 %bitcast_add_fusion = f32[16,2,20,2048]{3,0,2,1:T(8,128)S(1)} fusion(f32[16,2,20,2048]{3,0,2,1:T(8,128)} %collective-permute-done, f32[16,2,1,20,2048]{4,3,2,1,0:T(8,128)} %get-tuple-element.5), kind=kLoop, calls=%fused_computation.2 | loop fusion | flops 1310720 | bytes 15728640 | tf_op jit(solution)/shard_map/add | solution.py:53
  196.9 2.3 copy-done
  199.2 1.7 constant_dynamic-slice_fusion.2
  200.9 58.5 %collective-permute-done.1 = f32[16,1,20,2048]{3,0,2,1:T(8,128)S(1)} collective-permute-done((f32[16,1,20,2048]{3,0,2,1:T(8,128)}, f32[16,1,20,2048]{3,0,2,1:T(8,128)S(1)}, u32[]{:S(2)}, u32[]{:S(2)}) %collective-permute-start.1) | collective-permute-done | bytes 2621472 | tf_op jit(solution)/shard_map/ppermute | solution.py:10
  259.4 2.1 fusion.5
  261.5 1.9 copy.32
  263.4 5.7 %all-to-all-start.1 = ((bf16[16,20,2048]{2,1,0:T(8,128)(2,1)}), bf16[16,20,2048]{2,1,0:T(8,128)(2,1)S(1)}, u32[]{:S(2)}, u32[]{:S(2)}) async-start(bf16[16,20,2048]{2,1,0:T(8,128)(2,1)} %copy.32), calls=%async_computation.1 | async-start | bytes 3145728 | tf_op jit(solution)/shard_map/all_to_all | solution.py:55
  269.1 36.1 %all-to-all-done.1 = bf16[16,20,2048]{2,1,0:T(8,128)(2,1)S(1)} async-done(((bf16[16,20,2048]{2,1,0:T(8,128)(2,1)}), bf16[16,20,2048]{2,1,0:T(8,128)(2,1)S(1)}, u32[]{:S(2)}, u32[]{:S(2)}) %all-to-all-start.1) | async-done | bytes 1310752 | tf_op jit(solution)/shard_map/all_to_all | solution.py:55
  305.5 1.4 gather_fusion
  306.9 1.3 reshape.81
  308.2 3.9 %multiply_reduce_fusion = bf16[128,2048]{1,0:T(8,128)(2,1)} fusion(f32[128,2,2048]{2,1,0:T(2,128)S(1)} %reshape.81, f32[128,2]{1,0:T(8,128)S(1)} %copy.25), kind=kLoop, calls=%fused_computation.11 | loop fusion | flops 786432 | bytes 2622464 | tf_op jit(solution)/shard_map/reduce_sum | solution.py:58
  (24 shorter events, 5.0 us)
Async XLA Ops:
  12.5 121.5 %all-to-all-start = ((bf16[16,80,2048]{2,1,0:T(8,128)(2,1)}), bf16[16,80,2048]{2,1,0:T(8,128)(2,1)}, u32[]{:S(2)}, u32[]{:S(2)}) async-start(bf16[16,80,2048]{2,1,0:T(8,128)(2,1)} %bitcast.27), calls=%async_computation | async-start | bytes 10485760 | tf_op jit(solution)/shard_map/all_to_all | solution.py:35
  133.9 8.7 %copy-start.2 = (bf16[1,2048,896]{2,1,0:T(8,128)(2,1)S(1)}, bf16[1,2048,896]{2,1,0:T(8,128)(2,1)}, u32[]{:S(2)}) copy-start(bf16[1,2048,896]{2,1,0:T(8,128)(2,1)} %param.12) | copy-start | bytes 11010052
  180.2 9.0 %collective-permute-start = (f32[16,2,20,2048]{3,0,2,1:T(8,128)}, f32[16,2,20,2048]{3,0,2,1:T(8,128)}, u32[]{:S(2)}, u32[]{:S(2)}) collective-permute-start(f32[16,2,20,2048]{3,0,2,1:T(8,128)} %bitcast.26), channel_id=1, source_target_pairs={{0,1},{1,0},{2,3},{3,2},{4,5},{5,4},{6,7},{7,6},{8,9},{9,8},{10,11... | collective-permute-start | bytes 15728648 | tf_op jit(solution)/shard_map/ppermute | solution.py:10
  196.9 2.3 copy-start
  200.9 58.5 %collective-permute-start.1 = (f32[16,1,20,2048]{3,0,2,1:T(8,128)}, f32[16,1,20,2048]{3,0,2,1:T(8,128)S(1)}, u32[]{:S(2)}, u32[]{:S(2)}) collective-permute-start(f32[16,1,20,2048]{3,0,2,1:T(8,128)} %constant_dynamic-slice_fusion.2), channel_id=1, source_target_pairs={{0,2},{1,3},{2,0},{3,1},{4,6},{5,7},{6,4},{7,5},{8,10},{9,11},{10,... | collective-permute-start | bytes 7864328 | tf_op jit(solution)/shard_map/ppermute | solution.py:10
  261.4 7.6 %copy-start.1 = (f32[128,2]{0,1:T(2,128)S(1)}, f32[128,2]{0,1:T(2,128)}, u32[]{:S(2)}) copy-start(f32[128,2]{0,1:T(2,128)} %param.9) | copy-start | bytes 3076
  263.4 41.8 %all-to-all-start.1 = ((bf16[16,20,2048]{2,1,0:T(8,128)(2,1)}), bf16[16,20,2048]{2,1,0:T(8,128)(2,1)S(1)}, u32[]{:S(2)}, u32[]{:S(2)}) async-start(bf16[16,20,2048]{2,1,0:T(8,128)(2,1)} %copy.32), calls=%async_computation.1 | async-start | bytes 3145728 | tf_op jit(solution)/shard_map/all_to_all | solution.py:55
where the time goes:
time: 313 us; the launch traced here: 312 us
  waiting for transfers between devices  218 us (70%)
  local copies, waits for them, and re-layouts  33.6 us (11%)
  matrix products  28.6 us (9%)
  other arithmetic  19.1 us (6%)
  starting transfers between devices  12.3 us (4%)
    all_to_all x1, waiting for transfers between devices, per_device(): lax.all_to_all(copies.reshape(devices, capacity, model_width), 'ep', spli...  115 us
    ppermute x2, waiting for transfers between devices, partner(): lax.ppermute(x, axis, [(i, i ^ 1 << distance) for i in range(lax.axis_siz...  67.4 us
    all_to_all x1, waiting for transfers between devices, per_device(): lax.all_to_all(finished, 'ep', split_axis=0, concat_axis=0, tiled=True)  36.1 us
    dot_general x1, matrix products, per_device(): jnp.dot(hidden, w_down[0], preferred_element_type=jnp.float32)  11.1 us
    dynamic_slice x1, local copies, waits for them, and re-layouts, per_device(): kept_part = lax.dynamic_index_in_dim(halves, own_bit, 2, keepdims=False)  8.85 us
    dot_general x1, matrix products, per_device(): up_act = jnp.dot(expert_rows, w_up[0], preferred_element_type=jnp.float32)  8.76 us
    dot_general x1, matrix products, per_device(): jnp.dot(expert_rows, w_gate[0], preferred_element_type=jnp.float32)  8.73 us
    add x1, other arithmetic, per_device(): summed = kept_part + partner(given_part, 'ep', bit_index)  7.71 us
  transfers between devices with their start and end apart: 4, of which 4 were waited for; matrix products, arithmetic and copies ran while one was open for 0% of the time, Pallas kernels for 0%

commit v1 on v0

v1 whole, which is shorter than its diff:
```python
import functools

import jax
import jax.numpy as jnp
from jax import lax
from jax.experimental import pallas as pl
from jax.experimental.pallas import tpu as pltpu
from jax.sharding import PartitionSpec as P

GROUP = 4
LANE = 128


def kernel(n, cap, tok, rt, gt, gain, wg, wu, wd, out,
           normed, outgoing, xbuf, wgu, wdn, hidden, part, give, take, cross, crossed,
           finished, ret, total, w_sem, zs, zr, ys, yr, cs, cr, fs, fr, gs, gr, bs, br, es, er):
    toks, width = tok.shape
    ff = wg.shape[1]
    me = lax.axis_index("ep")
    g, j = me // GROUP, me % GROUP
    partner = g * GROUP + (j + 1 - 2 * (j % 2))
    across = g * GROUP + (j + 2) % GROUP
    sign = jnp.where(g < n // 2, 1, -1)
    offsets = list(range(n // 2, n)) + list(range(n // 2 - 1, 0, -1))

    def peer(offset):
        return (g + sign * offset + n) % n

    sources = [g] + [peer(o) for o in offsets]

    def remote(src, dst, send, recv, device):
        return pltpu.make_async_remote_copy(
            src_ref=src, dst_ref=dst, send_sem=send, recv_sem=recv,
            device_id={"ep": device}, device_id_type=pl.DeviceIdType.MESH)

    barrier = pltpu.get_barrier_semaphore()
    others = [partner, across] + [s * GROUP + j for s in sources[1:]]
    for other in others:
        pl.semaphore_signal(barrier, inc=1, device_id={"ep": other},
                            device_id_type=pl.DeviceIdType.MESH)

    tiles = ff // LANE
    loads = []
    for t in range(tiles):
        loads.append(pltpu.make_async_copy(wg.at[:, pl.ds(t * LANE, LANE)], wgu.at[t, :, pl.ds(0, LANE)], w_sem.at[2 * t]))
        loads.append(pltpu.make_async_copy(wu.at[:, pl.ds(t * LANE, LANE)], wgu.at[t, :, pl.ds(LANE, LANE)], w_sem.at[2 * t + 1]))
    loads.append(pltpu.make_async_copy(wd, wdn, w_sem.at[2 * tiles]))
    for load in loads:
        load.start()

    values = tok[...].astype(jnp.float32)
    scale = lax.rsqrt(jnp.mean(values * values, axis=-1, keepdims=True) + 1e-06)
    normed[...] = (values * scale * gain[...].astype(jnp.float32)).astype(jnp.bfloat16)

    first, second = rt[:, 0:1], rt[:, 1:2]
    experts_at = lax.broadcasted_iota(jnp.int32, (toks, LANE), 1)
    named = ((experts_at == first) | (experts_at == second)).astype(jnp.float32)
    lower = (lax.broadcasted_iota(jnp.int32, (toks, toks), 1)
             < lax.broadcasted_iota(jnp.int32, (toks, toks), 0)).astype(jnp.bfloat16)
    before = jnp.dot(lower, named.astype(jnp.bfloat16), preferred_element_type=jnp.float32)
    code = jnp.where(named > 0.5, before, -1.0)
    code_t = code.T

    def pack(e, dst):
        row = jnp.sum(jnp.where(lax.broadcasted_iota(jnp.int32, (LANE, toks), 0) == e, code_t, 0.0), axis=0, keepdims=True)
        slot = lax.broadcasted_iota(jnp.int32, (cap, toks), 0).astype(jnp.float32)
        pick = (slot == row).astype(jnp.bfloat16)

        def body(t, _):
            cols = pl.ds(pl.multiple_of(t * 512, 512), 512)
            dst[:, cols] = jnp.dot(pick, normed[:, cols], preferred_element_type=jnp.float32).astype(jnp.bfloat16)
            return _

        lax.fori_loop(0, width // 512, body, 0)

    def lane_rows(lane):
        return pl.ds(lane * cap, cap)

    waits = []

    def share_copies(i):
        s = sources[i]
        return [remote(xbuf.at[s, lane_rows(0)], xbuf.at[s, lane_rows(2)], ys.at[i], yr.at[i], across),
                remote(xbuf.at[s, lane_rows(0)], xbuf.at[s, lane_rows(1)], cs.at[i], cr.at[i], partner)]

    def forward_copy(i):
        s = sources[i]
        return remote(xbuf.at[s, lane_rows(2)], xbuf.at[s, lane_rows(3)], fs.at[i], fr.at[i], partner)

    def give_copy(i):
        return remote(give.at[i], take.at[i], gs.at[i], gr.at[i], partner)

    def cross_copy(i):
        return remote(cross.at[i], crossed.at[i], bs.at[i], br.at[i], across)

    def arrive(i):
        if i:
            s = sources[i]
            remote(outgoing.at[0], xbuf.at[s, lane_rows(0)], zs.at[0], zr.at[s], partner).wait_recv()
        for copy in share_copies(i):
            copy.start()
            waits.append(copy)

    def forward(i):
        share_copies(i)[0].wait_recv()
        copy = forward_copy(i)
        copy.start()
        waits.append(copy)

    def compute(i):
        s, slot = sources[i], i % 2
        share_copies(i)[1].wait_recv()
        forward_copy(i).wait_recv()

        def up(t, _):
            both = jnp.dot(xbuf[s], wgu[t], preferred_element_type=jnp.float32)
            gate_act, up_act = both[:, :LANE], both[:, LANE:]
            act = gate_act / (1.0 + jnp.exp(-gate_act)) * up_act
            hidden[:, pl.ds(pl.multiple_of(t * LANE, LANE), LANE)] = act.astype(jnp.bfloat16)
            return _

        lax.fori_loop(0, tiles, up, 0)

        def down(t, _):
            cols = pl.ds(pl.multiple_of(t * 256, 256), 256)
            piece = jnp.dot(hidden[...], wdn[:, cols], preferred_element_type=jnp.float32)
            part[slot, 0, :, cols] = piece[0:cap]
            give[i, 0, :, cols] = piece[cap:2 * cap].astype(jnp.bfloat16)
            part[slot, 1, :, cols] = piece[2 * cap:3 * cap]
            give[i, 1, :, cols] = piece[3 * cap:4 * cap].astype(jnp.bfloat16)
            return _

        lax.fori_loop(0, width // 256, down, 0)
        copy = give_copy(i)
        copy.start()
        waits.append(copy)

    def reduce_pair(i):
        give_copy(i).wait_recv()
        cross[i] = (part[i % 2, 1] + take[i, 1].astype(jnp.float32)).astype(jnp.bfloat16)
        copy = cross_copy(i)
        copy.start()
        waits.append(copy)

    def finish(i):
        cross_copy(i).wait_recv()
        done = (part[i % 2, 0] + take[i, 0].astype(jnp.float32) + crossed[i].astype(jnp.float32)).astype(jnp.bfloat16)
        if i == 0:
            ret[g] = done
        else:
            finished[i] = done
            copy = remote(finished.at[i], ret.at[g], es.at[i], er.at[g], sources[i] * GROUP + j)
            copy.start()
            waits.append(copy)

    def mix(i):
        e = sources[i]
        if i:
            remote(finished.at[i], ret.at[e], es.at[i], er.at[e], partner).wait_recv()
        column = jnp.sum(jnp.where(experts_at == e, code, 0.0), axis=1, keepdims=True)
        slot = lax.broadcasted_iota(jnp.int32, (toks, cap), 1).astype(jnp.float32)
        pick = (slot == column).astype(jnp.bfloat16)
        gate = jnp.where(first == e, gt[:, 0:1], 0.0) + jnp.where(second == e, gt[:, 1:2], 0.0)

        def body(t, _):
            cols = pl.ds(pl.multiple_of(t * 512, 512), 512)
            term = gate * jnp.dot(pick, ret[e, :, cols], preferred_element_type=jnp.float32)
            if i:
                term = total[:, cols] + term
            if i == n - 1:
                out[:, cols] = term.astype(jnp.bfloat16)
            else:
                total[:, cols] = term
            return _

        lax.fori_loop(0, width // 512, body, 0)

    pack(g, xbuf.at[g, lane_rows(0)])
    pack(sources[1], outgoing.at[1])
    pl.semaphore_wait(barrier, len(others))
    arrive(0)
    for i in range(1, n):
        if i > 1:
            pack(sources[i], outgoing.at[i])
        copy = remote(outgoing.at[i], xbuf.at[g, lane_rows(0)], zs.at[i], zr.at[g], sources[i] * GROUP + j)
        copy.start()
        waits.append(copy)
    forward(0)
    arrive(1)
    for load in loads:
        load.wait()
    for i in range(n):
        compute(i)
        if i:
            finish(i - 1)
        reduce_pair(i)
        if i + 1 < n:
            forward(i + 1)
        if i + 2 < n:
            arrive(i + 2)
    mix(0)
    if n > 2:
        mix(1)
    finish(n - 1)
    for i in range(2 if n > 2 else 1, n):
        mix(i)
    for copy in waits:
        copy.wait_send()


def per_device(tokens, routing, gates, norm_gain, w_gate, w_up, w_down):
    toks, width = tokens.shape
    top = routing.shape[1]
    devices = lax.axis_size("ep")
    n = devices // GROUP
    cap = GROUP * (5 * toks * top // (4 * devices))
    cap = -(-cap // 16) * 16
    ff = w_gate.shape[2]
    bf, f32 = jnp.bfloat16, jnp.float32
    dma = pltpu.SemaphoreType.DMA((n,))
    vmem = pl.BlockSpec(memory_space=pltpu.VMEM)
    hbm = pl.BlockSpec(memory_space=pl.ANY)
    return pl.pallas_call(
        functools.partial(kernel, n, cap),
        out_shape=jax.ShapeDtypeStruct((toks, width), bf),
        in_specs=[vmem] * 4 + [hbm] * 3,
        out_specs=vmem,
        scratch_shapes=[
            pltpu.VMEM((toks, width), bf),
            pltpu.VMEM((n, cap, width), bf),
            pltpu.VMEM((n, GROUP * cap, width), bf),
            pltpu.VMEM((ff // LANE, width, 2 * LANE), bf),
            pltpu.VMEM((ff, width), bf),
            pltpu.VMEM((GROUP * cap, ff), bf),
            pltpu.VMEM((2, 2, cap, width), f32),
            pltpu.VMEM((n, 2, cap, width), bf),
            pltpu.VMEM((n, 2, cap, width), bf),
            pltpu.VMEM((n, cap, width), bf),
            pltpu.VMEM((n, cap, width), bf),
            pltpu.VMEM((n, cap, width), bf),
            pltpu.VMEM((n, cap, width), bf),
            pltpu.VMEM((toks, width), f32),
            pltpu.SemaphoreType.DMA((2 * (ff // LANE) + 1,)),
        ] + [dma] * 14,
        compiler_params=pltpu.CompilerParams(
            collective_id=0, has_side_effects=True, vmem_limit_bytes=62 * 1024 * 1024),
    )(tokens, routing, gates, norm_gain.reshape(1, width), w_gate.reshape(w_gate.shape[1:]),
      w_up.reshape(w_up.shape[1:]), w_down.reshape(w_down.shape[1:]))


def solution(mesh):
    placed = (
        P(("grp", "ep"), None),
        P(("grp", "ep"), None),
        P(("grp", "ep"), None),
        P(),
        P("ep", None, None),
        P("ep", None, None),
        P("ep", None, None),
    )
    return jax.shard_map(
        per_device, mesh=mesh, in_specs=placed, out_specs=P(("grp", "ep"), None), check_vma=False
    )
```

time: 313 us -> 102 us (0.33)
  waiting for transfers between devices: 218 us -> 0 us
  Pallas kernels: 0 us -> 95.9 us
  matrix products: 28.6 us -> 0 us
  local copies, waits for them, and re-layouts: 33.6 us -> 5.98 us
  other arithmetic: 19.1 us -> 0 us
  starting transfers between devices: 12.3 us -> 0 us
    all_to_all x2 -> x0, waiting for transfers between devices: 151 us -> none  [the longest x1 115 us: per_device(): lax.all_to_all(copies.reshape(devices, capacity, model_width), 'ep', spli...]
    pallas_call x0 -> x1, Pallas kernels: none -> 95.9 us  [per_device(): pl.pallas_call(functools.partial(kernel, n, cap), out_shape=jax.ShapeDtyp...]
    ppermute x2 -> x0, waiting for transfers between devices: 67.4 us -> none  [partner(): lax.ppermute(x, axis, [(i, i ^ 1 << distance) for i in range(lax.axis_siz...]
    dot_general x3 -> x0, matrix products: 28.6 us -> none  [the longest x1 11.1 us: per_device(): jnp.dot(hidden, w_down[0], preferred_element_type=jnp.float32)]
    dynamic_slice x2 -> x0, local copies, waits for them, and re-layouts: 14.2 us -> none  [the longest x1 8.85 us: per_device(): kept_part = lax.dynamic_index_in_dim(halves, own_bit, 2, keepdims=False)]
    all_to_all x2 -> x0, starting transfers between devices: 12.2 us -> none  [the longest x1 6.52 us: per_device(): lax.all_to_all(copies.reshape(devices, capacity, model_width), 'ep', spli...]
    add x2 -> x0, other arithmetic: 8.4 us -> none  [the longest x1 7.71 us: per_device(): summed = kept_part + partner(given_part, 'ep', bit_index)]
    reduce_sum x4 -> x0, other arithmetic: 6.57 us -> none  [the longest x1 3.93 us: per_device(): mixed = jnp.sum(gates[..., None] * picked.astype(jnp.float32), axis=1)]
  transfers between devices with their start and end apart: 4 -> 0, of which waited for: 4 -> 0; matrix products, arithmetic and copies ran while one was open for 0% -> 0% of each run, Pallas kernels for 0% -> 0%
where the time goes in v1:
time: 102 us
  Pallas kernels  95.9 us (94%)
  local copies, waits for them, and re-layouts  5.98 us (6%)
    pallas_call x1, Pallas kernels, per_device(): pl.pallas_call(functools.partial(kernel, n, cap), out_shape=jax.ShapeDtyp...  95.9 us
    unnamed x3, local copies, waits for them, and re-layouts  4.7 us

profile of v1, /device:TPU:13, one launch (start us, length us, event | category | flops | bytes accessed | tf_op | source)
XLA Modules:
  0.0 101.9 jit_solution(9770238110410121283)
XLA Ops:
  0.0 1.3 %reshape.12.gain = bf16[1,2048]{1,0:T(2,128)(2,1)} reshape(bf16[2048]{0:T(1024)(128)(2,1)} %param.10) | data formatting | bytes 8192 | tf_op jit(solution)/shard_map/reshape | solution.py:247
  1.3 1.4 %copy.8.rt = s32[128,2]{1,0:T(8,128)} copy(s32[128,2]{0,1:T(2,128)} %param.8) | data formatting | bytes 2048 | tf_op args[1]
  2.7 1.4 %copy.9.gt = f32[128,2]{1,0:T(8,128)} copy(f32[128,2]{0,1:T(2,128)} %param.9) | data formatting | bytes 2048 | tf_op args[2]
  4.1 95.9 %shard_map.73 = bf16[128,2048]{1,0:T(8,128)(2,1)} custom-call(bf16[128,2048]{1,0:T(8,128)(2,1)} %tok.1, s32[128,2]{1,0:T(8,128)} %copy.8.rt, f32[128,2]{1,0:T(8,128)} %copy.9.gt, bf16[1,2048]{1,0:T(2,128)(2,1)} %reshape.12.gain, bf16[2048,896]{1,0:T(8,128)(2,1)} %bitcast.3, bf16[2048,896]{1,0:T(8,128)(2,1)} %bitcast.4, bf16[896,2048]{1,0:T(8,128)(2,1)} %bitcast.5), custom_call_target="tpu_custom_call" | custom-call | tf_op jit(solution)/shard_map/pallas_call | solution.py:223
  100.0 1.9 %copy.11 = bf16[128,2048]{1,0:T(8,128)(2,1)} copy(bf16[128,2048]{1,0:T(8,128)(2,1)} %shard_map.73) | data formatting | bytes 1048576

commit v2 on v1

v2 whole, which is shorter than its diff:
```python
import functools

import jax
import jax.numpy as jnp
from jax import lax
from jax.experimental import pallas as pl
from jax.experimental.pallas import tpu as pltpu
from jax.sharding import PartitionSpec as P

GROUP = 4
LANE = 128
PIECES = 4


def kernel(n, cap, tok, rt, gt, gain, wg, wu, wd, out,
           normed, outgoing, xbuf, wgu, wdn, hidden, part, give, take, cross, crossed,
           finished, ret, total, table, w_sem, zs, zr, ys, yr, cs, cr, fs, fr, gs, gr, bs, br, es, er):
    toks, width = tok.shape
    ff = wg.shape[1]
    me = lax.axis_index("ep")
    g, j = me // GROUP, me % GROUP
    partner = g * GROUP + (j + 1 - 2 * (j % 2))
    across = g * GROUP + (j + 2) % GROUP
    sources = [(g + o) % n for o in range(n)]
    send_order = sorted(range(1, n), key=lambda o: min(o, n - o))
    span = width // PIECES

    def remote(src, dst, send, recv, device):
        return pltpu.make_async_remote_copy(
            src_ref=src, dst_ref=dst, send_sem=send, recv_sem=recv,
            device_id={"ep": device}, device_id_type=pl.DeviceIdType.MESH)

    barrier = pltpu.get_barrier_semaphore()
    others = [partner, across] + [s * GROUP + j for s in sources[1:]]
    for other in others:
        pl.semaphore_signal(barrier, inc=1, device_id={"ep": other},
                            device_id_type=pl.DeviceIdType.MESH)

    tiles = ff // LANE
    loads = []
    for t in range(tiles):
        loads.append(pltpu.make_async_copy(wg.at[:, pl.ds(t * LANE, LANE)], wgu.at[t, :, pl.ds(0, LANE)], w_sem.at[2 * t]))
        loads.append(pltpu.make_async_copy(wu.at[:, pl.ds(t * LANE, LANE)], wgu.at[t, :, pl.ds(LANE, LANE)], w_sem.at[2 * t + 1]))
    loads.append(pltpu.make_async_copy(wd, wdn, w_sem.at[2 * tiles]))
    for load in loads:
        load.start()

    values = tok[...].astype(jnp.float32)
    scale = lax.rsqrt(jnp.mean(values * values, axis=-1, keepdims=True) + 1e-06)
    normed[...] = (values * scale * gain[...].reshape(1, width).astype(jnp.float32)).astype(jnp.bfloat16)

    table[...] = jnp.zeros_like(table)
    table[0:2] = rt[...].astype(jnp.float32)
    table[2:4] = gt[...]
    turned = table[...].T
    first, second = turned[:, 0:1], turned[:, 1:2]
    experts_at = lax.broadcasted_iota(jnp.int32, (toks, LANE), 1).astype(jnp.float32)
    named = ((experts_at == first) | (experts_at == second)).astype(jnp.float32)
    lower = (lax.broadcasted_iota(jnp.int32, (toks, toks), 1)
             < lax.broadcasted_iota(jnp.int32, (toks, toks), 0)).astype(jnp.bfloat16)
    before = jnp.dot(lower, named.astype(jnp.bfloat16), preferred_element_type=jnp.float32)
    code = jnp.where(named > 0.5, before, -1.0)
    code_t = code.T

    def pack(e, dst):
        row = jnp.sum(jnp.where(lax.broadcasted_iota(jnp.int32, (LANE, toks), 0) == e, code_t, 0.0), axis=0, keepdims=True)
        slot = lax.broadcasted_iota(jnp.int32, (cap, toks), 0).astype(jnp.float32)
        pick = (slot == row).astype(jnp.bfloat16)

        def body(t, _):
            cols = pl.ds(pl.multiple_of(t * 512, 512), 512)
            dst[:, cols] = jnp.dot(pick, normed[:, cols], preferred_element_type=jnp.float32).astype(jnp.bfloat16)
            return _

        lax.fori_loop(0, width // 512, body, 0)

    def lane_rows(lane):
        return pl.ds(lane * cap, cap)

    waits = []

    def start(copy):
        copy.start()
        waits.append(copy)

    def across_copy(i):
        s = sources[i]
        return remote(xbuf.at[s, lane_rows(0)], xbuf.at[s, lane_rows(2)], ys.at[i], yr.at[i], across)

    def beside_copy(i):
        s = sources[i]
        return remote(xbuf.at[s, lane_rows(0)], xbuf.at[s, lane_rows(1)], cs.at[i], cr.at[i], partner)

    def forward_copy(i):
        s = sources[i]
        return remote(xbuf.at[s, lane_rows(2)], xbuf.at[s, lane_rows(3)], fs.at[i], fr.at[i], partner)

    def piece_of(h):
        return pl.ds(h * span, span)

    def give_copy(i, h):
        return remote(give.at[i, :, :, piece_of(h)], take.at[i, :, :, piece_of(h)],
                      gs.at[i, h], gr.at[i, h], partner)

    def cross_copy(i, h):
        return remote(cross.at[i, :, piece_of(h)], crossed.at[i, :, piece_of(h)],
                      bs.at[i, h], br.at[i, h], across)

    def arrive(i):
        if i:
            s = sources[i]
            remote(outgoing.at[0], xbuf.at[s, lane_rows(0)], zs.at[0], zr.at[s], partner).wait_recv()
        start(across_copy(i))
        start(beside_copy(i))

    def forward(i):
        across_copy(i).wait_recv()
        start(forward_copy(i))

    def rise(i):
        s = sources[i]
        beside_copy(i).wait_recv()
        forward_copy(i).wait_recv()

        def up(t, _):
            both = jnp.dot(xbuf[s], wgu[t], preferred_element_type=jnp.float32)
            gate_act, up_act = both[:, :LANE], both[:, LANE:]
            act = gate_act / (1.0 + jnp.exp(-gate_act)) * up_act
            hidden[:, pl.ds(pl.multiple_of(t * LANE, LANE), LANE)] = act.astype(jnp.bfloat16)
            return _

        lax.fori_loop(0, tiles, up, 0)

    def fall(i, h):
        slot = i % 2

        def down(t, _):
            cols = pl.ds(pl.multiple_of(h * span + t * 256, 256), 256)
            piece = jnp.dot(hidden[...], wdn[:, cols], preferred_element_type=jnp.float32)
            part[slot, 0, :, cols] = piece[0:cap]
            give[i, 0, :, cols] = piece[cap:2 * cap].astype(jnp.bfloat16)
            part[slot, 1, :, cols] = piece[2 * cap:3 * cap]
            give[i, 1, :, cols] = piece[3 * cap:4 * cap].astype(jnp.bfloat16)
            return _

        lax.fori_loop(0, span // 256, down, 0)
        start(give_copy(i, h))

    def reduce_pair(i, h):
        give_copy(i, h).wait_recv()
        cols = piece_of(h)
        cross[i, :, cols] = (part[i % 2, 1, :, cols] + take[i, 1, :, cols].astype(jnp.float32)).astype(jnp.bfloat16)
        start(cross_copy(i, h))

    def finish(i, h):
        cross_copy(i, h).wait_recv()
        cols = piece_of(h)
        done = (part[i % 2, 0, :, cols] + take[i, 0, :, cols].astype(jnp.float32)
                + crossed[i, :, cols].astype(jnp.float32)).astype(jnp.bfloat16)
        if i == 0:
            ret[g, :, cols] = done
        else:
            finished[i, :, cols] = done
            start(remote(finished.at[i, :, cols], ret.at[g, :, cols], es.at[i, h], er.at[g, h],
                         sources[i] * GROUP + j))

    def mix(i, h, last):
        e = sources[i]
        cols = piece_of(h)
        if i:
            remote(finished.at[i, :, cols], ret.at[e, :, cols], es.at[i, h], er.at[e, h], partner).wait_recv()
        column = jnp.sum(jnp.where(experts_at == e.astype(jnp.float32), code, 0.0), axis=1, keepdims=True)
        slot = lax.broadcasted_iota(jnp.int32, (toks, cap), 1).astype(jnp.float32)
        pick = (slot == column).astype(jnp.bfloat16)
        name = e.astype(jnp.float32)
        gate = jnp.where(first == name, turned[:, 2:3], 0.0) + jnp.where(second == name, turned[:, 3:4], 0.0)
        term = gate * jnp.dot(pick, ret[e, :, cols], preferred_element_type=jnp.float32)
        if i:
            term = total[:, cols] + term
        if last:
            out[:, cols] = term.astype(jnp.bfloat16)
        else:
            total[:, cols] = term

    pieces = range(PIECES)
    pack(g, xbuf.at[g, lane_rows(0)])
    pack(sources[send_order[0]], outgoing.at[send_order[0]])
    pl.semaphore_wait(barrier, len(others))
    arrive(0)
    for o in send_order:
        if o != send_order[0]:
            pack(sources[o], outgoing.at[o])
        start(remote(outgoing.at[o], xbuf.at[g, lane_rows(0)], zs.at[o], zr.at[g], sources[o] * GROUP + j))
    forward(0)
    arrive(1)
    for load in loads:
        load.wait()
    for i in range(n):
        rise(i)
        if i and i + 1 < n:
            arrive(i + 1)
        for h in pieces:
            fall(i, h)
            if h:
                reduce_pair(i, h - 1)
        reduce_pair(i, PIECES - 1)
        if i:
            for h in pieces:
                finish(i - 1, h)
        if i + 1 < n:
            forward(i + 1)
    order = [0] + [n - o for o in range(1, n)]
    for i in order[:-1]:
        if i == order[-2]:
            for h in pieces:
                finish(n - 1, h)
        for h in pieces:
            mix(i, h, False)
    for h in pieces:
        mix(order[-1], h, True)
    for copy in waits:
        copy.wait_send()


def per_device(tokens, routing, gates, norm_gain, w_gate, w_up, w_down):
    toks, width = tokens.shape
    top = routing.shape[1]
    devices = lax.axis_size("ep")
    n = devices // GROUP
    cap = GROUP * (5 * toks * top // (4 * devices))
    cap = -(-cap // 16) * 16
    ff = w_gate.shape[2]
    bf, f32 = jnp.bfloat16, jnp.float32
    dma = pltpu.SemaphoreType.DMA((n,))
    dmas = pltpu.SemaphoreType.DMA((n, PIECES))
    vmem = pl.BlockSpec(memory_space=pltpu.VMEM)
    hbm = pl.BlockSpec(memory_space=pl.ANY)
    return pl.pallas_call(
        functools.partial(kernel, n, cap),
        out_shape=jax.ShapeDtypeStruct((toks, width), bf),
        in_specs=[vmem] * 4 + [hbm] * 3,
        out_specs=vmem,
        scratch_shapes=[
            pltpu.VMEM((toks, width), bf),
            pltpu.VMEM((n, cap, width), bf),
            pltpu.VMEM((n, GROUP * cap, width), bf),
            pltpu.VMEM((ff // LANE, width, 2 * LANE), bf),
            pltpu.VMEM((ff, width), bf),
            pltpu.VMEM((GROUP * cap, ff), bf),
            pltpu.VMEM((2, 2, cap, width), f32),
            pltpu.VMEM((n, 2, cap, width), bf),
            pltpu.VMEM((n, 2, cap, width), bf),
            pltpu.VMEM((n, cap, width), bf),
            pltpu.VMEM((n, cap, width), bf),
            pltpu.VMEM((n, cap, width), bf),
            pltpu.VMEM((n, cap, width), bf),
            pltpu.VMEM((toks, width), f32),
            pltpu.VMEM((LANE, toks), f32),
            pltpu.SemaphoreType.DMA((2 * (ff // LANE) + 1,)),
        ] + [dma] * 8 + [dmas] * 6,
        compiler_params=pltpu.CompilerParams(
            collective_id=0, has_side_effects=True, vmem_limit_bytes=62 * 1024 * 1024),
    )(tokens, routing.T, gates.T, norm_gain, w_gate.reshape(w_gate.shape[1:]),
      w_up.reshape(w_up.shape[1:]), w_down.reshape(w_down.shape[1:]))


def solution(mesh):
    placed = (
        P(("grp", "ep"), None),
        P(("grp", "ep"), None),
        P(("grp", "ep"), None),
        P(),
        P("ep", None, None),
        P("ep", None, None),
        P("ep", None, None),
    )
    return jax.shard_map(
        per_device, mesh=mesh, in_specs=placed, out_specs=P(("grp", "ep"), None), check_vma=False
    )
```

time: 102 us -> 95.4 us (0.935)
  local copies, waits for them, and re-layouts: 5.98 us -> 1.88 us
  Pallas kernels: 95.9 us -> 92.8 us
    pallas_call x1, Pallas kernels: 95.9 us -> 92.8 us  [per_device(): pl.pallas_call(functools.partial(kernel, n, cap), out_shape=jax.ShapeDtyp...]
    unnamed x3 -> x1, local copies, waits for them, and re-layouts: 4.7 us -> 1.88 us
    reshape x1 -> x0, local copies, waits for them, and re-layouts: 1.29 us -> none  [per_device(): norm_gain.reshape(1, width)]
where the time goes in v2:
time: 95.4 us; the launch traced here: 94.7 us
  Pallas kernels  92.8 us (97%)
  local copies, waits for them, and re-layouts  1.88 us (2%)
    pallas_call x1, Pallas kernels, per_device(): pl.pallas_call(functools.partial(kernel, n, cap), out_shape=jax.ShapeDtyp...  92.8 us

profile of v2, /device:TPU:13, one launch (start us, length us, event | category | flops | bytes accessed | tf_op | source)
XLA Modules:
  0.0 94.7 jit_solution(11416333181633820590)
XLA Ops:
  0.0 92.8 %shard_map.73 = bf16[128,2048]{1,0:T(8,128)(2,1)} custom-call(bf16[128,2048]{1,0:T(8,128)(2,1)} %tok.1, s32[2,128]{1,0:T(2,128)} %bitcast.8, f32[2,128]{1,0:T(2,128)} %bitcast.9, bf16[2048]{0:T(1024)(128)(2,1)} %gain.1, bf16[2048,896]{1,0:T(8,128)(2,1)} %bitcast.5, bf16[2048,896]{1,0:T(8,128)(2,1)} %bitcast.6, bf16[896,2048]{1,0:T(8,128)(2,1)} %bitcast.7), custom_call_target="tpu_custom_call" | custom-call | tf_op jit(solution)/shard_map/pallas_call | solution.py:238
  92.8 1.9 %copy.9 = bf16[128,2048]{1,0:T(8,128)(2,1)} copy(bf16[128,2048]{1,0:T(8,128)(2,1)} %shard_map.73) | data formatting | bytes 1048576
